TPU v7x, 32 devices: a whole 2x2x4 slice. The times are simulated.
32 devices in a mesh: rep: 2 (over x), fs: 8 (over z, y), tp: 2 (over core).
Axes of the slice: x: 2, y: 2, z: 4, core: 2. Of those that a mesh axis runs over, the one named last changes fastest.
Arguments:
- tokens: bfloat16 [4096, 2048], P(('rep', 'fs')), may hold values from -6 to 6
- mid_tokens: bfloat16 [4096, 2048], P(('rep', 'fs')), may hold values from -6 to 6
- out_grad: bfloat16 [4096, 2048], P(('rep', 'fs')), may hold values from -6 to 6
- gate_first: bfloat16 [2048, 3072], P('fs', 'tp'), may hold values from -0.125 to 0.125
- up_first: bfloat16 [2048, 3072], P('fs', 'tp'), may hold values from -0.125 to 0.125
- down_first: bfloat16 [3072, 2048], P('tp', 'fs'), may hold values from -0.109375 to 0.109375
- gate_second: bfloat16 [2048, 3072], P('fs', 'tp'), may hold values from -0.125 to 0.125
- up_second: bfloat16 [2048, 3072], P('fs', 'tp'), may hold values from -0.125 to 0.125
- down_second: bfloat16 [3072, 2048], P('tp', 'fs'), may hold values from -0.109375 to 0.109375
Outputs:
- input_grad: bfloat16 [4096, 2048], P(('rep', 'fs'))
- down_grad: float32 [3072, 2048], P('tp', 'fs')
- row_norms: float32 [3072], P('tp')
All inputs are finite; a program needn't handle non-finite values.
Results may differ from a plain program's by a relative error of at most 0.025.
Values may be sent and summed in bfloat16 or wider, within the bound.
A program may use at most 128 MiB of HBM per device.

v0:
```python
import jax
import jax.numpy as jnp
from jax import lax
from jax.sharding import PartitionSpec as P

eps = 1e-06


def half_back(field, carried, gate_w, up_w, down_w):
    scale = lax.rsqrt(jnp.mean(field * field, axis=1, keepdims=True) + eps)
    normed = field * scale
    normed_b = normed.astype(jnp.bfloat16)
    gates, uppers = (
        lax.all_gather(gate_w, "fs", axis=0, tiled=True),
        lax.all_gather(up_w, "fs", axis=0, tiled=True),
    )
    gate = jnp.dot(normed_b, gates, preferred_element_type=jnp.float32)
    upper = jnp.dot(normed_b, uppers, preferred_element_type=jnp.float32)
    back = 0.5 * lax.dot_general(
        carried,
        lax.all_gather(down_w, "fs", axis=1, tiled=True),
        (((1,), (1,)), ((), ())),
        preferred_element_type=jnp.float32,
    )
    logistic = jax.nn.sigmoid(gate)
    activated = gate * logistic
    hidden = (activated * upper).astype(jnp.bfloat16)
    d_gate = (back * upper * logistic * (1.0 + gate * (1.0 - logistic))).astype(jnp.bfloat16)
    d_up = (back * activated).astype(jnp.bfloat16)
    dims = (((1,), (1,)), ((), ()))
    partial_sum = lax.dot_general(d_gate, gates, dims, preferred_element_type=jnp.float32)
    partial_sum = partial_sum + lax.dot_general(
        d_up, uppers, dims, preferred_element_type=jnp.float32
    )
    d_normed = lax.psum(partial_sum.astype(jnp.bfloat16), "tp").astype(jnp.float32)
    d_field = carried.astype(jnp.float32) + scale * (
        d_normed - normed * jnp.mean(d_normed * normed, axis=1, keepdims=True)
    )
    return (d_field, hidden)


def on_device(
    tokens,
    mid_tokens,
    out_grad,
    gate_first,
    up_first,
    down_first,
    gate_second,
    up_second,
    down_second,
):
    d_mid, unused = half_back(
        mid_tokens.astype(jnp.float32), out_grad, gate_second, up_second, down_second
    )
    mid_grad = d_mid.astype(jnp.bfloat16)
    d_input, hidden = half_back(
        tokens.astype(jnp.float32), mid_grad, gate_first, up_first, down_first
    )
    owned = lax.all_to_all(mid_grad, "fs", split_axis=1, concat_axis=0, tiled=True)
    grad_shard = 0.5 * lax.dot_general(
        lax.all_gather(hidden, "fs", axis=0, tiled=True),
        owned,
        (((0,), (0,)), ((), ())),
        preferred_element_type=jnp.float32,
    )
    grad_shard = lax.psum(grad_shard.astype(jnp.bfloat16), "rep").astype(jnp.float32)
    norms = lax.psum(jnp.sum(grad_shard * grad_shard, axis=1), "fs")
    return (d_input.astype(jnp.bfloat16), grad_shard, norms)


def solution(mesh):
    placed = (
        P(("rep", "fs"), None),
        P(("rep", "fs"), None),
        P(("rep", "fs"), None),
        P("fs", "tp"),
        P("fs", "tp"),
        P("tp", "fs"),
        P("fs", "tp"),
        P("fs", "tp"),
        P("tp", "fs"),
    )
    return jax.shard_map(
        on_device,
        mesh=mesh,
        in_specs=placed,
        out_specs=(P(("rep", "fs"), None), P("tp", "fs"), P("tp")),
        check_vma=False,
    )
```

profile of v0, /device:TPU:0, one launch (start us, length us, event | category | flops | bytes accessed | tf_op | source)
XLA Modules:
  0.0 841.8 jit_solution(1562090629637954430)
XLA Ops:
  10.9 101.3 %all-gather.8.cloned.1.call-done = bf16[1536,2048]{1,0:T(8,128)(2,1)} async-done(((bf16[1536,256]{1,0:T(8,128)(2,1)}), bf16[1536,2048]{1,0:T(8,128)(2,1)}) %all-gather.8.cloned.1.call-update) | async-done | bytes 6291472 | tf_op jit(solution)/shard_map/all_gather | solution.py:21
  112.3 5.8 convolution_multiply_fusion.3
  118.0 93.3 %all-gather.12.cloned.1.call-done = bf16[2048,1536]{1,0:T(8,128)(2,1)} async-done(((bf16[256,1536]{1,0:T(8,128)(2,1)}), bf16[2048,1536]{1,0:T(8,128)(2,1)}) %all-gather.12.cloned.1.call-update) | async-done | bytes 6291472 | tf_op jit(solution)/shard_map/all_gather | solution.py:14
  211.3 5.8 fusion.25
  217.1 93.3 %all-gather.10.cloned.1.call-done = bf16[2048,1536]{1,0:T(8,128)(2,1)} async-done(((bf16[256,1536]{1,0:T(8,128)(2,1)}), bf16[2048,1536]{1,0:T(8,128)(2,1)}) %all-gather.10.cloned.1.call-update) | async-done | bytes 6291472 | tf_op jit(solution)/shard_map/all_gather | solution.py:15
  310.4 10.4 %fusion.24 = f32[256,2048]{1,0:T(8,128)} fusion(bf16[2048,1536]{1,0:T(8,128)(2,1)} %all-gather.12.cloned.1.call-done, f32[256,1536]{1,0:T(8,128)} %convolution_multiply_fusion.3, bf16[2048,1536]{1,0:T(8,128)(2,1)} %all-gather.10.cloned.1.call-done, f32[256,1536]{1,0:T(8,128)} %fusion.25, bf16[256,2048]{1,0:T(8,128)(2,1)S(1)} %copy-done, ...), kind=kOutput, calls=%fused_computation.46 | convolution fusion | flops 3226730496 | bytes 18875392 | tf_op jit(solution)/shard_map/dot_general | solution.py:31
  320.9 7.1 fusion.7
  329.5 79.9 %all-gather.18.cloned.1.call-done = bf16[2048,1536]{1,0:T(8,128)(2,1)} async-done(((bf16[256,1536]{1,0:T(8,128)(2,1)}), bf16[2048,1536]{1,0:T(8,128)(2,1)}) %all-gather.18.cloned.1.call-update) | async-done | bytes 6291472 | tf_op jit(solution)/shard_map/all_gather | solution.py:14
  409.4 5.8 fusion.29
  415.2 93.2 %all-gather.16.cloned.1.call-done = bf16[2048,1536]{1,0:T(8,128)(2,1)} async-done(((bf16[256,1536]{1,0:T(8,128)(2,1)}), bf16[2048,1536]{1,0:T(8,128)(2,1)}) %all-gather.16.cloned.1.call-update) | async-done | bytes 6291472 | tf_op jit(solution)/shard_map/all_gather | solution.py:15
  508.3 6.5 multiply_convert_fusion
  514.8 13.9 %all-reduce.4.cloned.1.call-done = bf16[256,2048]{1,0:T(8,128)(2,1)} async-done(((bf16[256,2048]{1,0:T(8,128)(2,1)}), bf16[256,2048]{1,0:T(8,128)(2,1)}) %all-reduce.4.cloned.1.call-update) | async-done | bytes 1048592 | tf_op jit(solution)/shard_map/psum | solution.py:35
  530.6 1.9 fusion.14
  533.5 5.8 all-to-all-start
  539.3 113.0 %all-gather.14.cloned.1.call-done = bf16[1536,2048]{1,0:T(8,128)(2,1)} async-done(((bf16[1536,256]{1,0:T(8,128)(2,1)}), bf16[1536,2048]{1,0:T(8,128)(2,1)}) %all-gather.14.cloned.1.call-update) | async-done | bytes 6291472 | tf_op jit(solution)/shard_map/all_gather | solution.py:21
  652.4 4.8 convolution_multiply_fusion.1
  657.1 5.1 fusion.21
  662.3 2.8 fusion.8
  665.4 86.0 %all-gather.20.cloned.1.call-done = bf16[2048,1536]{1,0:T(8,128)(2,1)} async-done(((bf16[256,1536]{1,0:T(8,128)(2,1)}), bf16[2048,1536]{1,0:T(8,128)(2,1)}) %all-gather.20.cloned.1.call-update) | async-done | bytes 6291472 | tf_op jit(solution)/shard_map/all_gather | solution.py:62
  751.4 5.5 fusion.9
  757.0 15.0 %all-reduce.6.cloned.1.call-done = bf16[256,2048]{1,0:T(8,128)(2,1)} async-done(((bf16[256,2048]{1,0:T(8,128)(2,1)}), bf16[256,2048]{1,0:T(8,128)(2,1)}) %all-reduce.6.cloned.1.call-update) | async-done | bytes 1048592 | tf_op jit(solution)/shard_map/psum | solution.py:35
  775.4 34.9 %all-reduce.8.cloned.1.call-done = bf16[1536,256]{1,0:T(8,128)(2,1)} async-done(((bf16[1536,256]{1,0:T(8,128)(2,1)}), bf16[1536,256]{1,0:T(8,128)(2,1)}) %all-reduce.8.cloned.1.call-update) | async-done | bytes 786448 | tf_op jit(solution)/shard_map/psum | solution.py:67
  810.3 2.4 multiply_reduce_fusion
  812.7 22.2 %psum.31 = f32[1536]{0:T(1024)} all-reduce(f32[1536]{0:T(1024)S(1)} %get-tuple-element.3), channel_id=1, replica_groups=mesh['rep'=2,'fs'=8,'tp'=2] {'fs'}, use_global_device_ids=true, to_apply=%region_8.0 | all-reduce | flops 1536 | bytes 12288 | tf_op jit(solution)/shard_map/psum | solution.py:68
  (50 shorter events, 11.8 us)
Async XLA Ops:
  7.2 3.5 copy-start
  7.2 105.1 %all-gather.8.cloned.1.call-start = ((), (), s32[]{:S(2)}) async-start(), calls=%async_computation.1 | async-start | bytes 7077888 | tf_op jit(solution)/shard_map/all_gather | solution.py:21
  7.9 104.4 %copy-start.4 = (bf16[256,2048]{1,0:T(8,128)(2,1)S(1)}, bf16[256,2048]{1,0:T(8,128)(2,1)}, u32[]{:S(2)}) copy-start(bf16[256,2048]{1,0:T(8,128)(2,1)} %param.11) | copy-start | bytes 3145732
  7.9 203.4 %all-gather.12.cloned.1.call-start = ((), (), s32[]{:S(2)}) async-start(), calls=%async_computation.3 | async-start | bytes 7077888 | tf_op jit(solution)/shard_map/all_gather | solution.py:14
  8.7 301.8 %all-gather.10.cloned.1.call-start = ((), (), s32[]{:S(2)}) async-start(), calls=%async_computation.2 | async-start | bytes 7077888 | tf_op jit(solution)/shard_map/all_gather | solution.py:15
  9.4 400.0 %all-gather.18.cloned.1.call-start = ((), (), s32[]{:S(2)}) async-start(), calls=%async_computation.7 | async-start | bytes 7077888 | tf_op jit(solution)/shard_map/all_gather | solution.py:14
  10.0 498.3 %all-gather.16.cloned.1.call-start = ((), (), s32[]{:S(2)}) async-start(), calls=%async_computation.6 | async-start | bytes 7077888 | tf_op jit(solution)/shard_map/all_gather | solution.py:15
  10.6 518.2 %all-reduce.4.cloned.1.call-start = ((), (), s32[]{:S(2)}) async-start(), calls=%async_computation.4 | async-start | bytes 2097152 | tf_op jit(solution)/shard_map/psum | solution.py:35
  328.0 1.2 copy-start.1
  328.0 324.3 %all-gather.14.cloned.1.call-start = ((), (), s32[]{:S(2)}) async-start(), calls=%async_computation.5 | async-start | bytes 7077888 | tf_op jit(solution)/shard_map/all_gather | solution.py:21
  328.8 422.6 %all-gather.20.cloned.1.call-start = ((), (), s32[]{:S(2)}) async-start(), calls=%async_computation.9 | async-start | bytes 7077888 | tf_op jit(solution)/shard_map/all_gather | solution.py:62
  528.7 1.8 copy-start.2
  533.5 131.9 %all-to-all-start = ((bf16[256,8,256]{2,0,1:T(8,128)(2,1)}), bf16[256,8,256]{2,0,1:T(8,128)(2,1)S(1)}, u32[]{:S(2)}, u32[]{:S(2)}) async-start(bf16[256,8,256]{2,0,1:T(8,128)(2,1)} %bitcast.20), calls=%async_computation | async-start | bytes 2097152 | tf_op jit(solution)/shard_map/all_to_all | solution.py:60
  539.3 232.7 %all-reduce.6.cloned.1.call-start = ((), (), s32[]{:S(2)}) async-start(), calls=%async_computation.8 | async-start | bytes 2097152 | tf_op jit(solution)/shard_map/psum | solution.py:35
  652.3 4.8 copy-start.5
  652.3 4.8 copy-start.6
  652.3 9.9 %slice-start = ((s8[6291456]{0:T(1024)(128)(4,1)}), s8[4194304]{0:T(1024)(128)(4,1)S(1)}, s32[]{:S(2)}) async-start(s8[6291456]{0:T(1024)(128)(4,1)} %bitcast.23), calls=%async_computation.11 | async-start | bytes 8388608
  657.1 5.1 slice-start.1
  665.1 145.2 %all-reduce.8.cloned.1.call-start = ((), (), s32[]{:S(2)}) async-start(), calls=%async_computation.10 | async-start | bytes 1572864 | tf_op jit(solution)/shard_map/psum | solution.py:67
  772.0 1.8 copy-start.3
Sparse Core Ops, SparseCore 0:
  10.0 102.1 all-gather.7
  114.4 96.8 all-gather.11
  213.5 96.8 all-gather.9
  312.5 96.8 all-gather.17
  411.4 96.8 all-gather.15
  511.1 17.6 all-reduce.3
  530.8 121.5 all-gather.13
  654.5 96.8 all-gather.19
  754.4 17.6 all-reduce.5
  774.7 35.5 all-reduce.7
where the time goes:
time: 842 us
  waiting for transfers between devices  728 us (86%)
  matrix products  59.5 us (7%)
  blocking collectives  22.2 us (3%)
  between operations  14.3 us (2%)
  other arithmetic  10.1 us (1%)
    all_gather x2, waiting for transfers between devices, half_back(): lax.all_gather(down_w, 'fs', axis=1, tiled=True)  214 us
    all_gather x2, waiting for transfers between devices, half_back(): lax.all_gather(up_w, 'fs', axis=0, tiled=True)  187 us
    all_gather x2, waiting for transfers between devices, half_back(): lax.all_gather(gate_w, 'fs', axis=0, tiled=True)  173 us
    all_gather x1, waiting for transfers between devices, on_device(): lax.all_gather(hidden, 'fs', axis=0, tiled=True)  86 us
    psum x1, waiting for transfers between devices, on_device(): lax.psum(grad_shard.astype(jnp.bfloat16), 'rep').astype(jnp.float32)  34.9 us
    psum x2, waiting for transfers between devices, half_back(): lax.psum(partial_sum.astype(jnp.bfloat16), 'tp').astype(jnp.float32)  29 us
    psum x1, blocking collectives, on_device(): norms = lax.psum(jnp.sum(grad_shard * grad_shard, axis=1), 'fs')  22.2 us
  transfers between devices with their start and end apart: 11, of which 10 were waited for; matrix products, arithmetic and copies ran while one was open for 8% of the time, Pallas kernels for 0%

commit v1 on v0

v1 whole, which is shorter than its diff:
```python
import jax
import jax.numpy as jnp
from jax import lax
from jax.sharding import PartitionSpec as P

eps = 1e-06


def gathered(gate_w, up_w, down_w):
    half = gate_w.shape[1] // lax.axis_size("rep")
    start = lax.axis_index("rep") * half
    own = jnp.concatenate(
        [
            lax.dynamic_slice_in_dim(gate_w, start, half, 1),
            lax.dynamic_slice_in_dim(up_w, start, half, 1),
            lax.dynamic_slice_in_dim(down_w, start, half, 0).T,
        ],
        axis=1,
    )
    return lax.all_gather(own, "fs", axis=0, tiled=True)


def half_back(field, fields, carried, carrieds, weights):
    half = weights.shape[1] // 3
    wide = fields.astype(jnp.float32)
    normed_b = (
        wide * lax.rsqrt(jnp.mean(wide * wide, axis=1, keepdims=True) + eps)
    ).astype(jnp.bfloat16)
    gates, uppers, downs = (weights[:, i * half : (i + 1) * half] for i in range(3))
    gate = jnp.dot(normed_b, gates, preferred_element_type=jnp.float32)
    upper = jnp.dot(normed_b, uppers, preferred_element_type=jnp.float32)
    back = 0.5 * jnp.dot(carrieds, downs, preferred_element_type=jnp.float32)
    logistic = jax.nn.sigmoid(gate)
    activated = gate * logistic
    hidden = (activated * upper).astype(jnp.bfloat16)
    d_gate = (back * upper * logistic * (1.0 + gate * (1.0 - logistic))).astype(jnp.bfloat16)
    d_up = (back * activated).astype(jnp.bfloat16)
    dims = (((1,), (1,)), ((), ()))
    partial_sum = lax.dot_general(d_gate, gates, dims, preferred_element_type=jnp.float32)
    partial_sum = partial_sum + lax.dot_general(
        d_up, uppers, dims, preferred_element_type=jnp.float32
    )
    partial_sum = partial_sum.astype(jnp.bfloat16)
    n = field.shape[0]
    reps = lax.axis_size("rep")
    me = lax.axis_index("rep")
    total = lax.dynamic_slice_in_dim(partial_sum, me * n, n, 0).astype(jnp.float32)
    for k in range(1, reps):
        other = lax.rem(me + k, reps)
        sent = lax.dynamic_slice_in_dim(partial_sum, other * n, n, 0)
        got = lax.ppermute(sent, "rep", [(i, (i + k) % reps) for i in range(reps)])
        total = total + got.astype(jnp.float32)
    d_normed = lax.psum(total.astype(jnp.bfloat16), "tp").astype(jnp.float32)
    own = field.astype(jnp.float32)
    scale = lax.rsqrt(jnp.mean(own * own, axis=1, keepdims=True) + eps)
    normed = own * scale
    d_field = carried.astype(jnp.float32) + scale * (
        d_normed - normed * jnp.mean(d_normed * normed, axis=1, keepdims=True)
    )
    return d_field.astype(jnp.bfloat16), hidden


def over_rep(x):
    return lax.all_gather(x, "rep", axis=0, tiled=True)


def on_device(tokens, mid_tokens, out_grad, gate_first, up_first, down_first, gate_second, up_second, down_second):
    second = gathered(gate_second, up_second, down_second)
    first = gathered(gate_first, up_first, down_first)
    mid_grad, _ = half_back(mid_tokens, over_rep(mid_tokens), out_grad, over_rep(out_grad), second)
    mid_grads = over_rep(mid_grad)
    d_input, hidden = half_back(tokens, over_rep(tokens), mid_grad, mid_grads, first)
    partial = lax.dot_general(
        mid_grads, hidden, (((0,), (0,)), ((), ())), preferred_element_type=jnp.float32
    )
    shard = lax.psum_scatter(
        (0.5 * partial).astype(jnp.bfloat16), "fs", scatter_dimension=0, tiled=True
    )
    grad = lax.all_gather(shard, "rep", axis=1, tiled=True).astype(jnp.float32)
    norms = lax.psum(jnp.sum(grad * grad, axis=0), "fs")
    return (d_input, grad.T, norms)


def solution(mesh):
    placed = (
        P(("rep", "fs"), None),
        P(("rep", "fs"), None),
        P(("rep", "fs"), None),
        P("fs", "tp"),
        P("fs", "tp"),
        P("tp", "fs"),
        P("fs", "tp"),
        P("fs", "tp"),
        P("tp", "fs"),
    )
    return jax.shard_map(
        on_device,
        mesh=mesh,
        in_specs=placed,
        out_specs=(P(("rep", "fs"), None), P("tp", "fs"), P("tp")),
        check_vma=False,
    )
```

time: 842 us -> 676 us (0.80)
  waiting for transfers between devices: 728 us -> 548 us
  blocking collectives: 22.2 us -> 31.5 us
    all_gather x7 -> x6, waiting for transfers between devices: 660 us -> 393 us  [the longest x2 276 us: gathered(): return lax.all_gather(own, 'fs', axis=0, tiled=True)]
    reduce_scatter x0 -> x1, waiting for transfers between devices: none -> 75.6 us  [on_device(): lax.psum_scatter((0.5 * partial).astype(jnp.bfloat16), 'fs', scatter_dime...]
    ppermute x0 -> x2, waiting for transfers between devices: none -> 49.1 us  [half_back(): got = lax.ppermute(sent, 'rep', [(i, (i + k) % reps) for i in range(reps)])]
    psum x3 -> x2, waiting for transfers between devices: 63.8 us -> 27.7 us  [half_back(): d_normed = lax.psum(total.astype(jnp.bfloat16), 'tp').astype(jnp.float32)]
    all_gather x0 -> x1, blocking collectives: none -> 11 us  [on_device(): grad = lax.all_gather(shard, 'rep', axis=1, tiled=True).astype(jnp.float32)]
  transfers between devices with their start and end apart: 11 -> 11, of which waited for: 10 -> 11; matrix products, arithmetic and copies ran while one was open for 8% -> 6% of each run, Pallas kernels for 0% -> 0%
where the time goes in v1:
time: 676 us; the launch traced here: 675 us
  waiting for transfers between devices  548 us (81%)
  matrix products  54.4 us (8%)
  blocking collectives  31.5 us (5%)
  other arithmetic  18.4 us (3%)
  between operations  14.1 us (2%)
  local copies, waits for them, and re-layouts  7.56 us (1%)
    all_gather x2, waiting for transfers between devices, gathered(): return lax.all_gather(own, 'fs', axis=0, tiled=True)  276 us
    all_gather x4, waiting for transfers between devices, over_rep(): return lax.all_gather(x, 'rep', axis=0, tiled=True)  117 us
    reduce_scatter x1, waiting for transfers between devices, on_device(): lax.psum_scatter((0.5 * partial).astype(jnp.bfloat16), 'fs', scatter_dime...  75.6 us
    ppermute x2, waiting for transfers between devices, half_back(): got = lax.ppermute(sent, 'rep', [(i, (i + k) % reps) for i in range(reps)])  49.1 us
    psum x2, waiting for transfers between devices, half_back(): d_normed = lax.psum(total.astype(jnp.bfloat16), 'tp').astype(jnp.float32)  27.7 us
    psum x1, blocking collectives, on_device(): norms = lax.psum(jnp.sum(grad * grad, axis=0), 'fs')  20.5 us
    dot_general x2, matrix products, half_back(): lax.dot_general(d_gate, gates, dims, preferred_element_type=jnp.float32)  13.9 us
  transfers between devices with their start and end apart: 11, of which 11 were waited for; matrix products, arithmetic and copies ran while one was open for 6% of the time, Pallas kernels for 0%

profile of v1, /device:TPU:0, one launch (start us, length us, event | category | flops | bytes accessed | tf_op | source)
XLA Modules:
  0.0 675.1 jit_solution(365070415602245520)
XLA Ops:
  11.5 33.9 %all-gather.11.cloned.1.call-done = bf16[512,2048]{1,0:T(8,128)(2,1)} async-done(((bf16[256,2048]{1,0:T(8,128)(2,1)}), bf16[512,2048]{1,0:T(8,128)(2,1)}) %all-gather.11.cloned.1.call-update) | async-done | bytes 2097168 | tf_op jit(solution)/shard_map/all_gather | solution.py:64
  47.6 138.2 %all-gather.7.cloned.1.call-done = bf16[2048,2304]{0,1:T(8,128)(2,1)} async-done(((bf16[256,2304]{0,1:T(8,128)(2,1)}), bf16[2048,2304]{0,1:T(8,128)(2,1)}) %all-gather.7.cloned.1.call-update) | async-done | bytes 9437200 | tf_op jit(solution)/shard_map/all_gather | solution.py:20
  185.8 4.9 fusion.17
  190.7 27.9 %all-gather.9.cloned.1.call-done = bf16[512,2048]{1,0:T(8,128)(2,1)} async-done(((bf16[256,2048]{1,0:T(8,128)(2,1)}), bf16[512,2048]{1,0:T(8,128)(2,1)}) %all-gather.9.cloned.1.call-update) | async-done | bytes 2097168 | tf_op jit(solution)/shard_map/all_gather | solution.py:64
  218.6 5.5 fusion.42
  224.1 9.8 %fusion.15 = f32[512,2048]{1,0:T(8,128)} fusion(bf16[2048,2304]{0,1:T(8,128)(2,1)} %all-gather.7.cloned.1.call-done, f32[768,512]{1,0:T(8,128)} %fusion.42, f32[512,768]{0,1:T(8,128)} %fusion.17, bf16[512,2048]{1,0:T(8,128)(2,1)S(1)} %copy-done.8, f32[512]{0:T(512)S(1)} %add_rsqrt_fusion.1), kind=kOutput, calls=%fused_computation.22 | convolution fusion | flops 3228303360 | bytes 15730688 | tf_op jit(solution)/shard_map/dot_general | solution.py:39
  233.9 6.0 add_convert_fusion.1
  241.3 24.7 %collective-permute-done = bf16[256,2048]{1,0:T(8,128)(2,1)} collective-permute-done((bf16[256,2048]{1,0:T(8,128)(2,1)}, bf16[256,2048]{1,0:T(8,128)(2,1)}, u32[]{:S(2)}, u32[]{:S(2)}) %collective-permute-start) | collective-permute-done | bytes 1048608 | tf_op jit(solution)/shard_map/ppermute | solution.py:51
  266.0 2.6 add_convert_fusion.3
  272.7 15.5 %all-reduce.3.cloned.1.call-done = bf16[256,2048]{1,0:T(8,128)(2,1)} async-done(((bf16[256,2048]{1,0:T(8,128)(2,1)}), bf16[256,2048]{1,0:T(8,128)(2,1)}) %all-reduce.3.cloned.1.call-update) | async-done | bytes 1048592 | tf_op jit(solution)/shard_map/psum | solution.py:53
  291.9 32.0 %all-gather.17.cloned.1.call-done = bf16[512,2048]{1,0:T(8,128)(2,1)} async-done(((bf16[256,2048]{1,0:T(8,128)(2,1)}), bf16[512,2048]{1,0:T(8,128)(2,1)}) %all-gather.17.cloned.1.call-update) | async-done | bytes 2097168 | tf_op jit(solution)/shard_map/all_gather | solution.py:64
  326.1 138.0 %all-gather.15.cloned.1.call-done = bf16[2048,2304]{0,1:T(8,128)(2,1)} async-done(((bf16[256,2304]{0,1:T(8,128)(2,1)}), bf16[2048,2304]{0,1:T(8,128)(2,1)}) %all-gather.15.cloned.1.call-update) | async-done | bytes 9437200 | tf_op jit(solution)/shard_map/all_gather | solution.py:20
  464.1 4.9 fusion.10
  469.0 5.2 fusion.13
  474.3 23.3 %all-gather.13.cloned.1.call-done = bf16[512,2048]{1,0:T(8,128)(2,1)} async-done(((bf16[256,2048]{1,0:T(8,128)(2,1)}), bf16[512,2048]{1,0:T(8,128)(2,1)}) %all-gather.13.cloned.1.call-update) | async-done | bytes 2097168 | tf_op jit(solution)/shard_map/all_gather | solution.py:64
  497.5 4.5 fusion.45
  502.0 4.1 fusion.8
  506.2 4.0 add_convert_fusion
  510.7 24.4 %collective-permute-done.1 = bf16[256,2048]{1,0:T(8,128)(2,1)S(1)} collective-permute-done((bf16[256,2048]{1,0:T(8,128)(2,1)S(1)}, bf16[256,2048]{1,0:T(8,128)(2,1)S(1)}, u32[]{:S(2)}, u32[]{:S(2)}) %collective-permute-start.1) | collective-permute-done | bytes 1048608 | tf_op jit(solution)/shard_map/ppermute | solution.py:51
  536.7 5.5 multiply_convert_fusion
  543.8 12.2 %all-reduce.5.cloned.1.call-done = bf16[256,2048]{1,0:T(8,128)(2,1)} async-done(((bf16[256,2048]{1,0:T(8,128)(2,1)}), bf16[256,2048]{1,0:T(8,128)(2,1)}) %all-reduce.5.cloned.1.call-update) | async-done | bytes 1048592 | tf_op jit(solution)/shard_map/psum | solution.py:53
  559.5 75.6 %reduce-scatter.2.cloned.1.call-done = bf16[256,768]{1,0:T(8,128)(2,1)} async-done(((bf16[2048,768]{1,0:T(8,128)(2,1)}), bf16[256,768]{1,0:T(8,128)(2,1)}) %reduce-scatter.2.cloned.1.call-update) | async-done | bytes 393232 | tf_op jit(solution)/shard_map/reduce_scatter | solution.py:76
  635.1 11.0 %all_gather.27 = bf16[256,1536]{1,0:T(8,128)(2,1)S(1)} all-gather(bf16[256,768]{1,0:T(8,128)(2,1)} %reduce-scatter.2.cloned.1.call-done), channel_id=1, replica_groups=mesh['rep'=2,'fs'=8,'tp'=2] {'rep'}, dimensions={1}, use_global_device_ids=true | all-gather | bytes 1179648 | tf_op jit(solution)/shard_map/all_gather | solution.py:79
  648.1 20.5 %psum.23 = f32[1536]{0:T(1024)} all-reduce(f32[1536]{0:T(1024)S(1)} %fusion.34), channel_id=1, replica_groups=mesh['rep'=2,'fs'=8,'tp'=2] {'fs'}, use_global_device_ids=true, to_apply=%region_10.0 | all-reduce | flops 1536 | bytes 12288 | tf_op jit(solution)/shard_map/psum | solution.py:80
  (78 shorter events, 26.9 us)
Async XLA Ops:
  7.2 2.3 copy-start
  7.2 38.2 %all-gather.11.cloned.1.call-start = ((), (), s32[]{:S(2)}) async-start(), calls=%async_computation.3 | async-start | bytes 3145728 | tf_op jit(solution)/shard_map/all_gather | solution.py:64
  7.9 177.9 %all-gather.7.cloned.1.call-start = ((), (), s32[]{:S(2)}) async-start(), calls=%async_computation.1 | async-start | bytes 10616832 | tf_op jit(solution)/shard_map/all_gather | solution.py:20
  10.7 208.0 %all-gather.9.cloned.1.call-start = ((), (), s32[]{:S(2)}) async-start(), calls=%async_computation.2 | async-start | bytes 3145728 | tf_op jit(solution)/shard_map/all_gather | solution.py:64
  11.4 276.8 %all-reduce.3.cloned.1.call-start = ((), (), s32[]{:S(2)}) async-start(), calls=%async_computation.4 | async-start | bytes 2097152 | tf_op jit(solution)/shard_map/psum | solution.py:53
  45.4 140.4 %copy-start.8 = (bf16[512,2048]{1,0:T(8,128)(2,1)S(1)}, bf16[512,2048]{1,0:T(8,128)(2,1)}, u32[]{:S(2)}) copy-start(bf16[512,2048]{1,0:T(8,128)(2,1)} %all-gather.11.cloned.1.call-done) | copy-start | bytes 6291460
  240.9 25.1 %collective-permute-start = (bf16[256,2048]{1,0:T(8,128)(2,1)}, bf16[256,2048]{1,0:T(8,128)(2,1)}, u32[]{:S(2)}, u32[]{:S(2)}) collective-permute-start(bf16[256,2048]{1,0:T(8,128)(2,1)} %constant_dynamic-slice_fusion.3), channel_id=1, source_target_pairs={{0,16},{16,0},{1,17},{17,1},{2,18},{18,2},{3,19},{19,3},{4,20},{20... | collective-permute-start | bytes 3145736 | tf_op jit(solution)/shard_map/ppermute | solution.py:51
  268.6 2.2 copy-start.10
  268.6 55.3 %all-gather.17.cloned.1.call-start = ((), (), s32[]{:S(2)}) async-start(), calls=%async_computation.7 | async-start | bytes 3145728 | tf_op jit(solution)/shard_map/all_gather | solution.py:64
  269.2 194.9 %all-gather.15.cloned.1.call-start = ((), (), s32[]{:S(2)}) async-start(), calls=%async_computation.6 | async-start | bytes 10616832 | tf_op jit(solution)/shard_map/all_gather | solution.py:20
  270.8 1.7 copy-start.2
  271.9 18.1 %copy-start.7 = (bf16[256,2048]{1,0:T(8,128)(2,1)S(1)}, bf16[256,2048]{1,0:T(8,128)(2,1)}, u32[]{:S(2)}) copy-start(bf16[256,2048]{1,0:T(8,128)(2,1)} %param.11) | copy-start | bytes 3145732
  271.9 225.6 %all-gather.13.cloned.1.call-start = ((), (), s32[]{:S(2)}) async-start(), calls=%async_computation.5 | async-start | bytes 3145728 | tf_op jit(solution)/shard_map/all_gather | solution.py:64
  288.2 1.8 copy-start.5
  291.6 264.4 %all-reduce.5.cloned.1.call-start = ((), (), s32[]{:S(2)}) async-start(), calls=%async_computation.8 | async-start | bytes 2097152 | tf_op jit(solution)/shard_map/psum | solution.py:53
  323.9 140.2 %copy-start.9 = (bf16[512,2048]{1,0:T(8,128)(2,1)S(1)}, bf16[512,2048]{1,0:T(8,128)(2,1)}, u32[]{:S(2)}) copy-start(bf16[512,2048]{1,0:T(8,128)(2,1)} %all-gather.17.cloned.1.call-done) | copy-start | bytes 6291460
  474.3 27.7 %copy-start.12 = (f32[512,768]{0,1:T(8,128)S(1)}, f32[512,768]{0,1:T(8,128)}, u32[]{:S(2)}) copy-start(f32[512,768]{0,1:T(8,128)} %fusion.10) | copy-start | bytes 4718596
  497.5 4.5 copy-start.13
  510.2 26.5 %copy-start.11 = (bf16[512,2048]{1,0:T(8,128)(2,1)S(1)}, bf16[512,2048]{1,0:T(8,128)(2,1)}, u32[]{:S(2)}) copy-start(bf16[512,2048]{1,0:T(8,128)(2,1)} %all-gather.13.cloned.1.call-done) | copy-start | bytes 6291460
  510.2 24.8 %collective-permute-start.1 = (bf16[256,2048]{1,0:T(8,128)(2,1)S(1)}, bf16[256,2048]{1,0:T(8,128)(2,1)S(1)}, u32[]{:S(2)}, u32[]{:S(2)}) collective-permute-start(bf16[256,2048]{1,0:T(8,128)(2,1)S(1)} %constant_dynamic-slice_fusion), channel_id=1, source_target_pairs={{0,16},{16,0},{1,17},{17,1},{2,18},{18,2},{3,19},{19,3},{4,20},{20... | collective-permute-start | bytes 3145736 | tf_op jit(solution)/shard_map/ppermute | solution.py:51
  536.5 98.7 %reduce-scatter.2.cloned.1.call-start = ((), (), s32[]{:S(2)}) async-start(), calls=%async_computation.9 | async-start | bytes 3538944 | tf_op jit(solution)/shard_map/reduce_scatter | solution.py:76
  543.5 14.4 %copy-start.4 = (bf16[256,2048]{1,0:T(8,128)(2,1)S(1)}, bf16[256,2048]{1,0:T(8,128)(2,1)}, u32[]{:S(2)}) copy-start(bf16[256,2048]{1,0:T(8,128)(2,1)} %fusion.28) | copy-start | bytes 3145732
  556.0 1.8 copy-start.6
  646.1 22.4 %copy-start.1 = (bf16[1536,256]{1,0:T(8,128)(2,1)S(1)}, bf16[1536,256]{1,0:T(8,128)(2,1)}, u32[]{:S(2)}) copy-start(bf16[1536,256]{1,0:T(8,128)(2,1)} %param.17) | copy-start | bytes 2359300
  (1 other events, 1.3 us)
Sparse Core Ops, SparseCore 0:
  9.5 35.8 all-gather.10
  48.0 137.7 all-gather.6
  187.3 31.2 all-gather.8
  268.7 19.4 all-reduce.2
  289.5 34.2 all-gather.16
  326.3 137.7 all-gather.14
  466.2 31.2 all-gather.12
  536.6 19.4 all-reduce.4
  559.6 75.4 reduce-scatter.1

commit v2 on v0

v2 whole, which is shorter than its diff:
```python
import functools

import jax
import jax.numpy as jnp
from jax import lax
from jax.experimental import pallas as pl
from jax.experimental.pallas import tpu as pltpu
from jax.sharding import PartitionSpec as P

eps = 1e-06
f32, bf16 = jnp.float32, jnp.bfloat16


def kernel(sizes, tok, mid, cot, w1, w2, out, grad, norms, full1, full2, toks, mids, cots, mgs, xb, hidden, d_gate, d_up, mgt, part, got1, snd2, got2, dn, rs_out, rs_in, gb, nb, w_send, w_recv, own_sem, x_send, x_recv, s1_send, s1_recv, s2_send, s2_recv, s3_send, s3_recv, r_send, r_recv, g_send, g_recv, n_send, n_recv):
    R, F, T, n, D, H, pieces = sizes
    S, half, C, width = D // F, D // F // 2, D // T, 3 * H // pieces
    r, f, t = (lax.axis_index(a) for a in ("rep", "fs", "tp"))

    def fs_at(position):
        q = lax.rem(position + 2 * F, F)
        hi = q // (F // 2)
        return (1 - hi) * 2 * q + hi * (2 * (F - 1 - q) + 1)

    odd = lax.rem(f, 2)
    p = (1 - odd) * (f // 2) + odd * (F - 1 - f // 2)
    side = (fs_at(p + 1), fs_at(p - 1))

    barrier = pltpu.get_barrier_semaphore()
    for axis, size, me in (("rep", R, r), ("fs", F, f), ("tp", T, t)):
        for k in range(1, size):
            pl.semaphore_signal(barrier, inc=1, device_id={axis: lax.rem(me + k, size)}, device_id_type=pl.DeviceIdType.MESH)
    pl.semaphore_wait(barrier, R + F + T - 3)

    def remote(src, dst, send, recv, **where):
        return pltpu.make_async_remote_copy(src_ref=src, dst_ref=dst, send_sem=send, recv_sem=recv, device_id=where, device_id_type=pl.DeviceIdType.MESH)

    fulls = (full1, full2)

    def shard(b, d, distance, piece):
        owner = fs_at(p - distance if d == 0 else p + distance)
        rows = pl.ds(pl.multiple_of(owner * S + d * half, half), half)
        return fulls[b].at[rows, pl.ds(pl.multiple_of(piece * width, 128), width)]

    def ring(b, d, distance, step, piece):
        ref = shard(b, d, distance, piece)
        return remote(ref, ref, w_send.at[b, d], w_recv.at[b, d, step, piece], fs=side[d])

    def start_ring(b):
        for piece in range(pieces):
            for d in (0, 1):
                ring(b, d, 0, 0, piece).start()

    def serve(b, lo, hi):
        @pl.loop(lo, hi)
        def _(k):
            step, piece = k // pieces, lax.rem(k, pieces)
            for d in (0, 1):
                ring(b, d, step + 1, step, piece).wait_recv()
                ring(b, d, step + 1, step + 1, piece).start()

    relays = (F - 2) * pieces

    def upto(count):
        return relays * count // 18

    def end_ring(b):
        for piece in range(pieces):
            for d in (0, 1):
                ring(b, d, F - 1, F - 2, piece).wait_recv()

    def drain(b):
        whole = fulls[b].at[pl.ds(0, (F - 1) * half)]
        for d in (0, 1):
            remote(whole, whole, w_send.at[b, d], w_recv.at[b, d, 0, 0], fs=side[d]).wait_send()

    mine = pl.ds(pl.multiple_of(r * n, n), n)
    pairs = (mids, cots, toks, mgs)
    held = pl.ds(pl.multiple_of(f * S, S), S)
    loads = [pltpu.make_async_copy(src, dst, own_sem.at[i]) for i, (src, dst) in enumerate(((w2, full2.at[held]), (mid, mids.at[mine]), (cot, cots.at[mine]), (tok, toks.at[mine]), (w1, full1.at[held])))]
    for c in loads:
        c.start()

    def swap(i):
        return [remote(pairs[i].at[mine], pairs[i].at[mine], x_send.at[i, k - 1], x_recv.at[i, k - 1], rep=lax.rem(r + k, R)) for k in range(1, R)]

    def swap_in(i):
        for k in range(1, R):
            rows = pl.ds(pl.multiple_of(lax.rem(r + R - k, R) * n, n), n)
            remote(pairs[i].at[rows], pairs[i].at[rows], x_send.at[i, k - 1], x_recv.at[i, k - 1], rep=lax.rem(r + k, R)).wait_recv()

    loads[0].wait()
    start_ring(1)
    for i in range(3):
        loads[i + 1].wait()
        for c in swap(i):
            c.start()
    loads[4].wait()

    def normalise(pair):
        @pl.loop(0, R * n // 32)
        def _(i):
            rows = pl.ds(pl.multiple_of(i * 32, 32), 32)
            u = pair[rows, :].astype(f32)
            xb[rows, :] = (u * lax.rsqrt(jnp.mean(u * u, axis=1, keepdims=True) + eps)).astype(bf16)

    chunk = 256 if H % 256 == 0 else 128

    def forward(full, c_ref):
        @pl.loop(0, H // chunk)
        def _(j):
            def cols(which):
                return pl.ds(pl.multiple_of(which * H + j * chunk, 128), chunk)

            gate = jnp.dot(xb[...], full[:, cols(0)], preferred_element_type=f32)
            upper = jnp.dot(xb[...], full[:, cols(1)], preferred_element_type=f32)
            back = 0.5 * jnp.dot(c_ref[...], full[:, cols(2)], preferred_element_type=f32)
            logistic = jax.nn.sigmoid(gate)
            activated = gate * logistic
            hidden[:, cols(0)] = (activated * upper).astype(bf16)
            d_gate[:, cols(0)] = (back * upper * logistic * (1.0 + gate * (1.0 - logistic))).astype(bf16)
            d_up[:, cols(0)] = (back * activated).astype(bf16)

    dims = (((1,), (1,)), ((), ()))

    def backward(full, lo, hi):
        @pl.loop(lo, hi)
        def _(j):
            rows = pl.ds(pl.multiple_of(j * 256, 256), 256)
            total = lax.dot_general(d_gate[...], full[rows, 0:H], dims, preferred_element_type=f32)
            total = total + lax.dot_general(d_up[...], full[rows, H : 2 * H], dims, preferred_element_type=f32)
            part[:, rows] = total.astype(bf16)

    def block_of(k):
        return pl.ds(pl.multiple_of(k * C, 128), C)

    def stage1(b):
        return [remote(part.at[:, block_of(lax.rem(t + k, T))], got1.at[b, k - 1], s1_send.at[b, k - 1], s1_recv.at[b, k - 1], tp=lax.rem(t + k, T)) for k in range(1, T)]

    def stage2(b):
        return [remote(snd2.at[k - 1], got2.at[b, k - 1], s2_send.at[b, k - 1], s2_recv.at[b, k - 1], rep=lax.rem(r + k, R)) for k in range(1, R)]

    def stage3(b, owner):
        ref = dn.at[b, :, block_of(owner)]
        return lambda k: remote(ref, ref, s3_send.at[b, k - 1], s3_recv.at[b, k - 1], tp=lax.rem(t + k, T))

    def summed(b, base, i):
        rows = pl.ds(pl.multiple_of(base * n + i * 32, 32), 32)
        total = part[rows, block_of(t)].astype(f32)
        for k in range(T - 1):
            total = total + got1[b, k, rows, :].astype(f32)
        return total

    def reduce_tp(b):
        for c in stage1(b):
            c.wait()
        for k in range(1, R):
            @pl.loop(0, n // 32)
            def _(i, k=k):
                snd2[k - 1, pl.ds(pl.multiple_of(i * 32, 32), 32), :] = summed(b, lax.rem(r + k, R), i).astype(bf16)
        for c in stage2(b):
            c.start()

    def reduce_rep(b):
        for c in stage2(b):
            c.wait()

        @pl.loop(0, n // 32)
        def _(i):
            rows = pl.ds(pl.multiple_of(i * 32, 32), 32)
            total = summed(b, r, i)
            for k in range(R - 1):
                total = total + got2[b, k, rows, :].astype(f32)
            dn[b, rows, block_of(t)] = total.astype(bf16)

        for k in range(1, T):
            stage3(b, t)(k).start()

    def finish(b, pair, carried, result, offset):
        for k in range(1, T):
            stage3(b, lax.rem(t + T - k, T))(k).wait_recv()
            stage3(b, t)(k).wait_send()

        @pl.loop(0, n // 32)
        def _(i):
            rows = pl.ds(pl.multiple_of(i * 32, 32), 32)
            wide = pl.ds(pl.multiple_of(r * n + i * 32, 32), 32)
            u = pair[wide, :].astype(f32)
            scale = lax.rsqrt(jnp.mean(u * u, axis=1, keepdims=True) + eps)
            normed = u * scale
            d = dn[b, rows, :].astype(f32)
            d_u = carried[wide, :].astype(f32) + scale * (d - normed * jnp.mean(d * normed, axis=1, keepdims=True))
            result[pl.ds(pl.multiple_of(offset + i * 32, 32), 32), :] = d_u.astype(bf16)

    serve(1, 0, upto(10))
    swap_in(0)
    normalise(mids)
    serve(1, upto(10), upto(18))
    start_ring(0)
    swap_in(1)
    end_ring(1)
    forward(full2, cots)
    serve(0, 0, upto(1))
    backward(full2, 0, D // 512)
    serve(0, upto(1), upto(2))
    backward(full2, D // 512, D // 256)
    for c in stage1(1):
        c.start()
    serve(0, upto(2), upto(4))
    reduce_tp(1)
    swap_in(2)
    normalise(toks)
    serve(0, upto(4), upto(7))
    reduce_rep(1)
    serve(0, upto(7), upto(8))
    finish(1, mids, cots, mgs, r * n)
    for c in swap(3):
        c.start()
    serve(0, upto(8), upto(17))
    swap_in(3)

    @pl.loop(0, D // 256)
    def _(j):
        cols = pl.ds(pl.multiple_of(j * 256, 256), 256)
        mgt[cols, :] = mgs[:, cols].T

    serve(0, upto(17), upto(18))
    end_ring(0)

    forward(full1, mgs)

    def product(d, position):
        rows = pl.ds(pl.multiple_of(fs_at(position) * S + d * half, half), half)
        return 0.5 * jnp.dot(mgt[rows, :], hidden[...], preferred_element_type=f32)

    def rs(d, s):
        return remote(rs_out.at[d, s], rs_in.at[d, s], r_send.at[d, s], r_recv.at[d, s], fs=side[d])

    def passed(lo, hi):
        @pl.loop(lo, hi)
        def _(s):
            for d in (0, 1):
                value = product(d, p - 1 - s if d == 0 else p + 1 + s)
                rs(d, s - 1).wait_recv()
                rs_out[d, s] = (value + rs_in[d, s - 1].astype(f32)).astype(bf16)
                rs(d, s).start()

    def hop(count):
        return 1 + (F - 2) * count // 6

    for d in (0, 1):
        rs_out[d, 0] = product(d, p - 1 if d == 0 else p + 1).astype(bf16)
        rs(d, 0).start()
    backward(full1, 0, D // 256)
    for c in stage1(0):
        c.start()
    passed(1, hop(1))
    reduce_tp(0)
    passed(hop(1), hop(4))
    reduce_rep(0)
    passed(hop(4), hop(5))
    finish(0, toks, mgs, out, 0)
    passed(hop(5), hop(6))
    for d in (0, 1):
        value = product(d, p)
        rs(d, F - 2).wait_recv()
        gb[r, pl.ds(d * half, half), :] = (value + rs_in[d, F - 2].astype(f32)).astype(bf16)

    def trade(owner):
        return lambda k: remote(gb.at[owner], gb.at[owner], g_send.at[k - 1], g_recv.at[k - 1], rep=lax.rem(r + k, R))

    for k in range(1, R):
        trade(r)(k).start()
    for k in range(1, R):
        trade(lax.rem(r + R - k, R))(k).wait_recv()
        trade(r)(k).wait_send()
    for k in range(R):
        g = gb[k].astype(f32)
        grad[:, k * H : (k + 1) * H] = g
        nb[f, :, k * H : (k + 1) * H] = jnp.sum(g * g, axis=0, keepdims=True)

    def tell(owner):
        return lambda k: remote(nb.at[owner], nb.at[owner], n_send.at[k - 1], n_recv.at[k - 1], fs=lax.rem(f + k, F))

    for k in range(1, F):
        tell(f)(k).start()
    for b in (0, 1):
        drain(b)
    for i in range(4):
        for c in swap(i):
            c.wait_send()

    @pl.loop(0, F - 1)
    def _(s):
        for d in (0, 1):
            rs(d, s).wait_send()

    for k in range(1, F):
        tell(lax.rem(f + F - k, F))(k).wait_recv()
        tell(f)(k).wait_send()
    total = nb[0]
    for k in range(1, F):
        total = total + nb[k]
    norms[...] = total


def on_device(sizes, tokens, mid_tokens, out_grad, gate_first, up_first, down_first, gate_second, up_second, down_second):
    R, F, T, n, D, H, pieces = sizes
    S, half = D // F, D // F // 2
    start = lax.axis_index("rep") * H

    def own(gate_w, up_w, down_w):
        return jnp.concatenate(
            [
                lax.dynamic_slice_in_dim(gate_w, start, H, 1),
                lax.dynamic_slice_in_dim(up_w, start, H, 1),
                lax.dynamic_slice_in_dim(down_w, start, H, 0).T,
            ],
            axis=1,
        )

    dma = pltpu.SemaphoreType.DMA
    m = R * n
    any_space = pl.BlockSpec(memory_space=pl.ANY)
    vmem = pl.BlockSpec(memory_space=pltpu.VMEM)
    d_input, grad, norms = pl.pallas_call(
        functools.partial(kernel, sizes),
        out_shape=(
            jax.ShapeDtypeStruct((n, D), bf16),
            jax.ShapeDtypeStruct((S, R * H), f32),
            jax.ShapeDtypeStruct((1, R * H), f32),
        ),
        in_specs=[any_space] * 5,
        out_specs=(vmem, vmem, vmem),
        scratch_shapes=[
            pltpu.VMEM((D, 3 * H), bf16),
            pltpu.VMEM((D, 3 * H), bf16),
            pltpu.VMEM((m, D), bf16),
            pltpu.VMEM((m, D), bf16),
            pltpu.VMEM((m, D), bf16),
            pltpu.VMEM((m, D), bf16),
            pltpu.VMEM((m, D), bf16),
            pltpu.VMEM((m, H), bf16),
            pltpu.VMEM((m, H), bf16),
            pltpu.VMEM((m, H), bf16),
            pltpu.VMEM((D, m), bf16),
            pltpu.VMEM((m, D), bf16),
            pltpu.VMEM((2, T - 1, m, D // T), bf16),
            pltpu.VMEM((R - 1, n, D // T), bf16),
            pltpu.VMEM((2, R - 1, n, D // T), bf16),
            pltpu.VMEM((2, n, D), bf16),
            pltpu.VMEM((2, F - 1, half, H), bf16),
            pltpu.VMEM((2, F - 1, half, H), bf16),
            pltpu.VMEM((R, S, H), bf16),
            pltpu.VMEM((F, 1, R * H), f32),
            dma((2, 2)),
            dma((2, 2, F - 1, pieces)),
            dma((5,)),
            dma((4, R - 1)),
            dma((4, R - 1)),
            dma((2, T - 1)),
            dma((2, T - 1)),
            dma((2, R - 1)),
            dma((2, R - 1)),
            dma((2, T - 1)),
            dma((2, T - 1)),
            dma((2, F - 1)),
            dma((2, F - 1)),
            dma((R - 1,)),
            dma((R - 1,)),
            dma((F - 1,)),
            dma((F - 1,)),
        ],
        compiler_params=pltpu.CompilerParams(
            collective_id=0, has_side_effects=True, vmem_limit_bytes=67043328
        ),
    )(
        tokens,
        mid_tokens,
        out_grad,
        own(gate_first, up_first, down_first),
        own(gate_second, up_second, down_second),
    )
    return d_input, grad.T, norms.reshape(-1)


def solution(mesh):
    R, F, T = (mesh.shape[a] for a in ("rep", "fs", "tp"))

    def whole(tokens, mid_tokens, out_grad, gate_first, *rest):
        D, FF = gate_first.shape
        sizes = (R, F, T, tokens.shape[0] // (R * F), D, FF // (T * R), 3 if F <= 8 else 1)
        return jax.shard_map(
            functools.partial(on_device, sizes),
            mesh=mesh,
            in_specs=(P(("rep", "fs"), None),) * 3 + (P("fs", "tp"), P("fs", "tp"), P("tp", "fs")) * 2,
            out_specs=(P(("rep", "fs"), None), P("tp", "fs"), P("tp")),
            check_vma=False,
        )(tokens, mid_tokens, out_grad, gate_first, *rest)

    return whole
```

time: 842 us -> 256 us (0.30)
  waiting for transfers between devices: 728 us -> 0 us
  Pallas kernels: 0 us -> 246 us
  matrix products: 59.5 us -> 0 us
  blocking collectives: 22.2 us -> 0 us
  between operations: 14.3 us -> 0.72 us
    all_gather x7 -> x0, waiting for transfers between devices: 660 us -> none  [the longest x2 214 us: half_back(): lax.all_gather(down_w, 'fs', axis=1, tiled=True)]
    pallas_call x0 -> x1, Pallas kernels: none -> 246 us  [on_device(): pl.pallas_call(functools.partial(kernel, sizes), out_shape=(jax.ShapeDtyp...]
    psum x3 -> x0, waiting for transfers between devices: 63.8 us -> none  [the longest x1 34.9 us: on_device(): lax.psum(grad_shard.astype(jnp.bfloat16), 'rep').astype(jnp.float32)]
    dot_general x10 -> x0, matrix products: 59.5 us -> none  [the longest x2 15.5 us: half_back(): lax.dot_general(d_gate, gates, dims, preferred_element_type=jnp.float32)]
    psum x1 -> x0, blocking collectives: 22.2 us -> none  [on_device(): norms = lax.psum(jnp.sum(grad_shard * grad_shard, axis=1), 'fs')]
  transfers between devices with their start and end apart: 11 -> 0, of which waited for: 10 -> 0; matrix products, arithmetic and copies ran while one was open for 8% -> 0% of each run, Pallas kernels for 0% -> 0%
where the time goes in v2:
time: 256 us
  Pallas kernels  246 us (96%)
  local copies, waits for them, and re-layouts  6.63 us (3%)
  other arithmetic  2.81 us (1%)
    pallas_call x1, Pallas kernels, on_device(): pl.pallas_call(functools.partial(kernel, sizes), out_shape=(jax.ShapeDtyp...  246 us
    unnamed x16, local copies, waits for them, and re-layouts  5.25 us

profile of v2, /device:TPU:0, one launch (start us, length us, event | category | flops | bytes accessed | tf_op | source)
XLA Modules:
  0.0 256.0 jit_solution(18139428631019461584)
XLA Ops:
  0.6 0.0 copy-start.1
  0.6 0.0 copy-start.2
  0.7 1.3 constant_dynamic-slice_fusion.4
  1.9 0.1 copy-done.1
  2.0 0.2 copy-done.2
  2.2 0.1 constant_dynamic-slice_fusion
  2.3 0.2 copy.16
  2.5 0.0 copy-start.3
  2.5 0.0 copy-start.4
  2.5 0.2 copy.15
  2.7 1.1 pad_maximum_fusion.w1
  3.8 0.0 copy-done.3
  3.8 0.5 copy-done.4
  4.3 0.1 constant_dynamic-slice_fusion.1
  4.3 1.1 pad_maximum_fusion.1.w2
  5.4 245.8 %shard_map.112 = (bf16[256,2048]{1,0:T(8,128)(2,1)}, f32[256,1536]{1,0:T(8,128)}, f32[1,1536]{1,0:T(1,128)}) custom-call(bf16[256,2048]{1,0:T(8,128)(2,1)} %tok.1, bf16[256,2048]{1,0:T(8,128)(2,1)} %mid.1, bf16[256,2048]{1,0:T(8,128)(2,1)} %cot.1, bf16[256,2304]{1,0:T(8,128)(2,1)} %pad_maximum_fusion.w1, bf16[256,2304]{1,0:T(8,128)(2,1)} %pad_maximum_fusion.1.w2), custom_call_target="tpu_custom_call" | custom-call | tf_op jit(solution)/shard_map/pallas_call | solution.py:325
  251.2 0.0 copy-start.5
  251.3 0.0 copy-start
  251.3 3.1 %copy.14 = f32[1536,256]{1,0:T(8,128)} copy(f32[1536,256]{0,1:T(8,128)} %bitcast.3) | data formatting | bytes 3145728
  254.4 0.0 copy-done.5
  254.4 0.6 reduce
  255.0 0.0 copy-done
  255.0 1.0 copy.18
Async XLA Ops:
  0.6 1.4 copy-start.1
  0.6 1.6 copy-start.2
  2.5 1.3 copy-start.3
  2.5 1.8 copy-start.4
  251.2 3.1 %copy-start.5 = (f32[1,1536]{1,0:T(1,128)S(1)}, f32[1,1536]{1,0:T(1,128)}, u32[]{:S(2)}) copy-start(f32[1,1536]{1,0:T(1,128)} %get-tuple-element.8) | copy-start | bytes 18436
  251.3 3.7 %copy-start = (bf16[256,2048]{1,0:T(8,128)(2,1)S(1)}, bf16[256,2048]{1,0:T(8,128)(2,1)}, u32[]{:S(2)}) copy-start(bf16[256,2048]{1,0:T(8,128)(2,1)} %get-tuple-element.21) | copy-start | bytes 3145732

commit v3 on v2

v3 whole, which is shorter than its diff:
```python
import functools

import jax
import jax.numpy as jnp
from jax import lax
from jax.experimental import pallas as pl
from jax.experimental.pallas import tpu as pltpu
from jax.sharding import PartitionSpec as P

eps = 1e-06
f32, bf16 = jnp.float32, jnp.bfloat16


def kernel(sizes, tok, mid, cot, w1, v1, w2, v2, out, grad, norms, full1, downs1, full2, downs2, toks, mids, cots, mgs, xb, hidden, d_gate, d_up, mgt, gates, uppers, part, got1, snd2, got2, dn, rs_out, rs_in, gb, nb, w_send, w_recv, own_sem, x_send, x_recv, s1_send, s1_recv, s2_send, s2_recv, s3_send, s3_recv, r_send, r_recv, g_send, g_recv, n_send, n_recv):
    R, F, T, n, D, H, pieces = sizes
    S, half, C, width = D // F, D // F // 2, D // T, H // pieces
    both = 2 if pieces > 1 else 1
    r, f, t = (lax.axis_index(a) for a in ("rep", "fs", "tp"))

    def fs_at(position):
        q = lax.rem(position + 2 * F, F)
        hi = q // (F // 2)
        return (1 - hi) * 2 * q + hi * (2 * (F - 1 - q) + 1)

    odd = lax.rem(f, 2)
    p = (1 - odd) * (f // 2) + odd * (F - 1 - f // 2)
    side = (fs_at(p + 1), fs_at(p - 1))

    barrier = pltpu.get_barrier_semaphore()
    for axis, size, me in (("rep", R, r), ("fs", F, f), ("tp", T, t)):
        for k in range(1, size):
            pl.semaphore_signal(barrier, inc=1, device_id={axis: lax.rem(me + k, size)}, device_id_type=pl.DeviceIdType.MESH)
    pl.semaphore_wait(barrier, R + F + T - 3)

    def remote(src, dst, send, recv, **where):
        return pltpu.make_async_remote_copy(src_ref=src, dst_ref=dst, send_sem=send, recv_sem=recv, device_id=where, device_id_type=pl.DeviceIdType.MESH)

    fulls = ((full1, downs1), (full2, downs2))

    second_gu, second_d = (1, 0, both, 2 * H // both, 0), (1, 1, pieces, width, both)
    first_gu, first_d = (0,) + second_gu[1:], (0,) + second_d[1:]

    def ring(phase, d, distance, step, piece):
        b, which, count, wide, sem = phase
        owner = fs_at(p - distance if d == 0 else p + distance)
        rows = pl.ds(pl.multiple_of(owner * S + d * half, half), half)
        ref = fulls[b][which].at[rows]
        if count > 1:
            ref = fulls[b][which].at[rows, pl.ds(pl.multiple_of(piece * wide, 128), wide)]
        return remote(ref, ref, w_send.at[b, which, d], w_recv.at[b, d, step, sem + piece], fs=side[d])

    def start_ring(phase):
        for piece in range(phase[2]):
            for d in (0, 1):
                ring(phase, d, 0, 0, piece).start()

    def serve(phase, lo, hi, of):
        relays = (F - 2) * phase[2]

        @pl.loop(relays * lo // of, relays * hi // of)
        def _(k):
            step, piece = k // phase[2], lax.rem(k, phase[2])
            for d in (0, 1):
                ring(phase, d, step + 1, step, piece).wait_recv()
                ring(phase, d, step + 1, step + 1, piece).start()

    def end_ring(phase):
        for piece in range(phase[2]):
            for d in (0, 1):
                ring(phase, d, F - 1, F - 2, piece).wait_recv()

    def drain(b):
        for which in (0, 1):
            whole = fulls[b][which].at[pl.ds(0, (F - 1) * half)]
            for d in (0, 1):
                remote(whole, whole, w_send.at[b, which, d], w_recv.at[b, d, 0, 0], fs=side[d]).wait_send()

    mine = pl.ds(pl.multiple_of(r * n, n), n)
    pairs = (mids, cots, toks, mgs)
    held = pl.ds(pl.multiple_of(f * S, S), S)
    loads = [pltpu.make_async_copy(src, dst, own_sem.at[i]) for i, (src, dst) in enumerate(((w2, full2.at[held]), (mid, mids.at[mine]), (cot, cots.at[mine]), (tok, toks.at[mine]), (v2, downs2.at[held]), (w1, full1.at[held]), (v1, downs1.at[held])))]
    for c in loads:
        c.start()

    def swap(i):
        return [remote(pairs[i].at[mine], pairs[i].at[mine], x_send.at[i, k - 1], x_recv.at[i, k - 1], rep=lax.rem(r + k, R)) for k in range(1, R)]

    def swap_in(i):
        for k in range(1, R):
            rows = pl.ds(pl.multiple_of(lax.rem(r + R - k, R) * n, n), n)
            remote(pairs[i].at[rows], pairs[i].at[rows], x_send.at[i, k - 1], x_recv.at[i, k - 1], rep=lax.rem(r + k, R)).wait_recv()

    loads[0].wait()
    start_ring(second_gu)
    for i in range(3):
        loads[i + 1].wait()
        for c in swap(i):
            c.start()
    for c in loads[4:]:
        c.wait()

    def normalise(pair):
        @pl.loop(0, R * n // 32)
        def _(i):
            rows = pl.ds(pl.multiple_of(i * 32, 32), 32)
            u = pair[rows, :].astype(f32)
            xb[rows, :] = (u * lax.rsqrt(jnp.mean(u * u, axis=1, keepdims=True) + eps)).astype(bf16)

    chunk = 256 if H % 256 == 0 else 128 if H % 128 == 0 else H

    def cols(which, j):
        if chunk == H:
            return pl.ds(which * H, H)
        return pl.ds(pl.multiple_of(which * H + j * chunk, 128), chunk)

    def forward(full):
        @pl.loop(0, H // chunk)
        def _(j):
            gate = jnp.dot(xb[...], full[:, cols(0, j)], preferred_element_type=f32)
            upper = jnp.dot(xb[...], full[:, cols(1, j)], preferred_element_type=f32)
            hidden[:, cols(0, j)] = (gate * jax.nn.sigmoid(gate) * upper).astype(bf16)
            gates[:, cols(0, j)] = gate
            uppers[:, cols(0, j)] = upper

    def backed(downs, c_ref):
        @pl.loop(0, H // chunk)
        def _(j):
            gate, upper = gates[:, cols(0, j)], uppers[:, cols(0, j)]
            back = 0.5 * jnp.dot(c_ref[...], downs[:, cols(0, j)], preferred_element_type=f32)
            logistic = jax.nn.sigmoid(gate)
            d_gate[:, cols(0, j)] = (back * upper * logistic * (1.0 + gate * (1.0 - logistic))).astype(bf16)
            d_up[:, cols(0, j)] = (back * gate * logistic).astype(bf16)

    dims = (((1,), (1,)), ((), ()))

    def backward(full, lo, hi):
        @pl.loop(lo, hi)
        def _(j):
            rows = pl.ds(pl.multiple_of(j * 256, 256), 256)
            total = lax.dot_general(d_gate[...], full[rows, 0:H], dims, preferred_element_type=f32)
            total = total + lax.dot_general(d_up[...], full[rows, H : 2 * H], dims, preferred_element_type=f32)
            part[:, rows] = total.astype(bf16)

    def block_of(k):
        return pl.ds(pl.multiple_of(k * C, 128), C)

    def stage1(b):
        return [remote(part.at[:, block_of(lax.rem(t + k, T))], got1.at[b, k - 1], s1_send.at[b, k - 1], s1_recv.at[b, k - 1], tp=lax.rem(t + k, T)) for k in range(1, T)]

    def stage2(b):
        return [remote(snd2.at[k - 1], got2.at[b, k - 1], s2_send.at[b, k - 1], s2_recv.at[b, k - 1], rep=lax.rem(r + k, R)) for k in range(1, R)]

    def stage3(b, owner):
        ref = dn.at[b, :, block_of(owner)]
        return lambda k: remote(ref, ref, s3_send.at[b, k - 1], s3_recv.at[b, k - 1], tp=lax.rem(t + k, T))

    def summed(b, base, i):
        rows = pl.ds(pl.multiple_of(base * n + i * 32, 32), 32)
        total = part[rows, block_of(t)].astype(f32)
        for k in range(T - 1):
            total = total + got1[b, k, rows, :].astype(f32)
        return total

    def reduce_tp(b):
        for c in stage1(b):
            c.wait()
        for k in range(1, R):
            @pl.loop(0, n // 32)
            def _(i, k=k):
                snd2[k - 1, pl.ds(pl.multiple_of(i * 32, 32), 32), :] = summed(b, lax.rem(r + k, R), i).astype(bf16)
        for c in stage2(b):
            c.start()

    def reduce_rep(b):
        for c in stage2(b):
            c.wait()

        @pl.loop(0, n // 32)
        def _(i):
            rows = pl.ds(pl.multiple_of(i * 32, 32), 32)
            total = summed(b, r, i)
            for k in range(R - 1):
                total = total + got2[b, k, rows, :].astype(f32)
            dn[b, rows, block_of(t)] = total.astype(bf16)

        for k in range(1, T):
            stage3(b, t)(k).start()

    def finish(b, pair, carried, result, offset):
        for k in range(1, T):
            stage3(b, lax.rem(t + T - k, T))(k).wait_recv()
            stage3(b, t)(k).wait_send()

        @pl.loop(0, n // 32)
        def _(i):
            rows = pl.ds(pl.multiple_of(i * 32, 32), 32)
            wide = pl.ds(pl.multiple_of(r * n + i * 32, 32), 32)
            u = pair[wide, :].astype(f32)
            scale = lax.rsqrt(jnp.mean(u * u, axis=1, keepdims=True) + eps)
            normed = u * scale
            d = dn[b, rows, :].astype(f32)
            d_u = carried[wide, :].astype(f32) + scale * (d - normed * jnp.mean(d * normed, axis=1, keepdims=True))
            result[pl.ds(pl.multiple_of(offset + i * 32, 32), 32), :] = d_u.astype(bf16)

    serve(second_gu, 0, 10, 12)
    swap_in(0)
    normalise(mids)
    serve(second_gu, 10, 12, 12)
    start_ring(second_d)
    end_ring(second_gu)
    serve(second_d, 0, 3, 18)
    forward(full2)
    serve(second_d, 3, 18, 18)
    start_ring(first_gu)
    swap_in(1)
    end_ring(second_d)
    backed(downs2, cots)
    serve(first_gu, 0, 1, 12)
    backward(full2, 0, D // 512)
    serve(first_gu, 1, 2, 12)
    backward(full2, D // 512, D // 256)
    for c in stage1(1):
        c.start()
    serve(first_gu, 2, 3, 12)
    reduce_tp(1)
    serve(first_gu, 3, 4, 12)
    swap_in(2)
    normalise(toks)
    serve(first_gu, 4, 6, 12)
    reduce_rep(1)
    serve(first_gu, 6, 7, 12)
    finish(1, mids, cots, mgs, r * n)
    for c in swap(3):
        c.start()
    serve(first_gu, 7, 12, 12)
    start_ring(first_d)
    end_ring(first_gu)

    forward(full1)
    serve(first_d, 0, 6, 18)
    swap_in(3)

    @pl.loop(0, D // 256)
    def _(j):
        part_cols = pl.ds(pl.multiple_of(j * 256, 256), 256)
        mgt[part_cols, :] = mgs[:, part_cols].T

    serve(first_d, 6, 18, 18)

    def strip(piece):
        return pl.ds(pl.multiple_of(piece * width, 128), width) if pieces > 1 else slice(None)

    def product(d, position, piece):
        rows = pl.ds(pl.multiple_of(fs_at(position) * S + d * half, half), half)
        return 0.5 * jnp.dot(mgt[rows, :], hidden[:, strip(piece)], preferred_element_type=f32)

    def view(ref, piece):
        return ref.at[:, strip(piece)] if pieces > 1 else ref

    def rs(d, s, piece):
        return remote(view(rs_out.at[d, s], piece), view(rs_in.at[d, s], piece), r_send.at[d, s, piece], r_recv.at[d, s, piece], fs=side[d])

    def passed(lo, hi):
        @pl.loop(1 + (F - 2) * lo // 6, 1 + (F - 2) * hi // 6)
        def _(s):
            for piece in range(pieces):
                for d in (0, 1):
                    value = product(d, p - 1 - s if d == 0 else p + 1 + s, piece)
                    rs(d, s - 1, piece).wait_recv()
                    rs_out[d, s, :, strip(piece)] = (value + rs_in[d, s - 1, :, strip(piece)].astype(f32)).astype(bf16)
                    rs(d, s, piece).start()

    for piece in range(pieces):
        for d in (0, 1):
            rs_out[d, 0, :, strip(piece)] = product(d, p - 1 if d == 0 else p + 1, piece).astype(bf16)
            rs(d, 0, piece).start()
    end_ring(first_d)
    backed(downs1, mgs)
    passed(0, 1)
    backward(full1, 0, D // 512)
    passed(1, 2)
    backward(full1, D // 512, D // 256)
    for c in stage1(0):
        c.start()
    passed(2, 3)
    reduce_tp(0)
    passed(3, 6)

    def trade(owner, piece):
        ref = view(gb.at[owner], piece)
        return lambda k: remote(ref, ref, g_send.at[k - 1, piece], g_recv.at[k - 1, piece], rep=lax.rem(r + k, R))

    for piece in range(pieces):
        for d in (0, 1):
            value = product(d, p, piece)
            rs(d, F - 2, piece).wait_recv()
            gb[r, pl.ds(d * half, half), strip(piece)] = (value + rs_in[d, F - 2, :, strip(piece)].astype(f32)).astype(bf16)
        for k in range(1, R):
            trade(r, piece)(k).start()
    reduce_rep(0)
    finish(0, toks, mgs, out, 0)
    for piece in range(pieces):
        for k in range(1, R):
            trade(lax.rem(r + R - k, R), piece)(k).wait_recv()
            trade(r, piece)(k).wait_send()
    for k in range(R):
        g = gb[k].astype(f32)
        grad[:, k * H : (k + 1) * H] = g
        nb[f, :, k * H : (k + 1) * H] = jnp.sum(g * g, axis=0, keepdims=True)

    def tell(owner):
        return lambda k: remote(nb.at[owner], nb.at[owner], n_send.at[k - 1], n_recv.at[k - 1], fs=lax.rem(f + k, F))

    for k in range(1, F):
        tell(f)(k).start()
    for b in (0, 1):
        drain(b)
    for i in range(4):
        for c in swap(i):
            c.wait_send()

    @pl.loop(0, F - 1)
    def _(s):
        for piece in range(pieces):
            for d in (0, 1):
                rs(d, s, piece).wait_send()

    for k in range(1, F):
        tell(lax.rem(f + F - k, F))(k).wait_recv()
        tell(f)(k).wait_send()
    total = nb[0]
    for k in range(1, F):
        total = total + nb[k]
    norms[...] = total


def on_device(sizes, tokens, mid_tokens, out_grad, gate_first, up_first, down_first, gate_second, up_second, down_second):
    R, F, T, n, D, H, pieces = sizes
    S, half = D // F, D // F // 2
    start = lax.axis_index("rep") * H

    def own(gate_w, up_w, down_w):
        pair = [lax.dynamic_slice_in_dim(w, start, H, 1) for w in (gate_w, up_w)]
        return jnp.concatenate(pair, axis=1), lax.dynamic_slice_in_dim(down_w, start, H, 0).T

    dma = pltpu.SemaphoreType.DMA
    m = R * n
    any_space = pl.BlockSpec(memory_space=pl.ANY)
    vmem = pl.BlockSpec(memory_space=pltpu.VMEM)
    d_input, grad, norms = pl.pallas_call(
        functools.partial(kernel, sizes),
        out_shape=(
            jax.ShapeDtypeStruct((n, D), bf16),
            jax.ShapeDtypeStruct((S, R * H), f32),
            jax.ShapeDtypeStruct((1, R * H), f32),
        ),
        in_specs=[any_space] * 7,
        out_specs=(vmem, vmem, vmem),
        scratch_shapes=[
            pltpu.VMEM((D, 2 * H), bf16),
            pltpu.VMEM((D, H), bf16),
            pltpu.VMEM((D, 2 * H), bf16),
            pltpu.VMEM((D, H), bf16),
            pltpu.VMEM((m, D), bf16),
            pltpu.VMEM((m, D), bf16),
            pltpu.VMEM((m, D), bf16),
            pltpu.VMEM((m, D), bf16),
            pltpu.VMEM((m, D), bf16),
            pltpu.VMEM((m, H), bf16),
            pltpu.VMEM((m, H), bf16),
            pltpu.VMEM((m, H), bf16),
            pltpu.VMEM((D, m), bf16),
            pltpu.VMEM((m, H), f32),
            pltpu.VMEM((m, H), f32),
            pltpu.VMEM((m, D), bf16),
            pltpu.VMEM((2, T - 1, m, D // T), bf16),
            pltpu.VMEM((R - 1, n, D // T), bf16),
            pltpu.VMEM((2, R - 1, n, D // T), bf16),
            pltpu.VMEM((2, n, D), bf16),
            pltpu.VMEM((2, F - 1, half, H), bf16),
            pltpu.VMEM((2, F - 1, half, H), bf16),
            pltpu.VMEM((R, S, H), bf16),
            pltpu.VMEM((F, 1, R * H), f32),
            dma((2, 2, 2)),
            dma((2, 2, F - 1, pieces + (2 if pieces > 1 else 1))),
            dma((7,)),
            dma((4, R - 1)),
            dma((4, R - 1)),
            dma((2, T - 1)),
            dma((2, T - 1)),
            dma((2, R - 1)),
            dma((2, R - 1)),
            dma((2, T - 1)),
            dma((2, T - 1)),
            dma((2, F - 1, pieces)),
            dma((2, F - 1, pieces)),
            dma((R - 1, pieces)),
            dma((R - 1, pieces)),
            dma((F - 1,)),
            dma((F - 1,)),
        ],
        compiler_params=pltpu.CompilerParams(
            collective_id=0, has_side_effects=True, vmem_limit_bytes=67043328
        ),
    )(
        tokens,
        mid_tokens,
        out_grad,
        *own(gate_first, up_first, down_first),
        *own(gate_second, up_second, down_second),
    )
    return d_input, grad.T, norms.reshape(-1)


def solution(mesh):
    R, F, T = (mesh.shape[a] for a in ("rep", "fs", "tp"))

    def whole(tokens, mid_tokens, out_grad, gate_first, *rest):
        D, FF = gate_first.shape
        sizes = (R, F, T, tokens.shape[0] // (R * F), D, FF // (T * R), 3 if F <= 8 and FF // (T * R) % 384 == 0 else 1)
        return jax.shard_map(
            functools.partial(on_device, sizes),
            mesh=mesh,
            in_specs=(P(("rep", "fs"), None),) * 3 + (P("fs", "tp"), P("fs", "tp"), P("tp", "fs")) * 2,
            out_specs=(P(("rep", "fs"), None), P("tp", "fs"), P("tp")),
            check_vma=False,
        )(tokens, mid_tokens, out_grad, gate_first, *rest)

    return whole
```

time: 256 us -> 247 us (0.965)
  Pallas kernels: 246 us -> 236 us
    pallas_call x1, Pallas kernels: 246 us -> 236 us  [on_device(): pl.pallas_call(functools.partial(kernel, sizes), out_shape=(jax.ShapeDtyp...]
where the time goes in v3:
time: 247 us; the launch traced here: 246 us
  Pallas kernels  236 us (96%)
  local copies, waits for them, and re-layouts  7.35 us (3%)
  other arithmetic  2.48 us (1%)
    pallas_call x1, Pallas kernels, on_device(): pl.pallas_call(functools.partial(kernel, sizes), out_shape=(jax.ShapeDtyp...  236 us
    unnamed x16, local copies, waits for them, and re-layouts  5.95 us

profile of v3, /device:TPU:0, one launch (start us, length us, event | category | flops | bytes accessed | tf_op | source)
XLA Modules:
  0.0 246.5 jit_solution(8580568673106795205)
XLA Ops:
  0.6 0.0 copy-start.1
  0.6 0.0 copy-start.2
  0.7 1.3 constant_dynamic-slice_fusion.4
  1.9 0.9 pad_maximum_fusion.w1
  2.9 0.0 copy-done.1
  2.9 0.0 copy-done.2
  2.9 0.0 copy-start.3
  2.9 0.0 copy-start.4
  2.9 0.1 constant_dynamic-slice_fusion
  3.0 0.9 copy.16
  3.9 0.9 copy.15
  4.8 0.0 copy-done.3
  4.8 0.0 copy-done.4
  4.8 0.1 constant_dynamic-slice_fusion.1
  4.9 0.9 pad_maximum_fusion.1.w2
  5.8 236.0 %shard_map.112 = (bf16[256,2048]{1,0:T(8,128)(2,1)}, f32[256,1536]{1,0:T(8,128)}, f32[1,1536]{1,0:T(1,128)}) custom-call(bf16[256,2048]{1,0:T(8,128)(2,1)} %tok.1, bf16[256,2048]{1,0:T(8,128)(2,1)} %mid.1, bf16[256,2048]{1,0:T(8,128)(2,1)} %cot.1, bf16[256,1536]{1,0:T(8,128)(2,1)} %pad_maximum_fusion.w1, bf16[256,768]{1,0:T(8,128)(2,1)} %bitcast.5, ...), custom_call_target="tpu_custom_call" | custom-call | tf_op jit(solution)/shard_map/pallas_call | solution.py:350
  241.8 0.0 copy-start.5
  241.8 0.0 copy-start
  241.8 3.1 %copy.14 = f32[1536,256]{1,0:T(8,128)} copy(f32[1536,256]{0,1:T(8,128)} %bitcast.3) | data formatting | bytes 3145728
  244.9 0.0 copy-done.5
  244.9 0.6 reduce
  245.5 0.0 copy-done
  245.5 1.0 copy.18
Async XLA Ops:
  0.6 2.2 copy-start.1
  0.6 2.2 copy-start.2
  2.9 1.9 copy-start.3
  2.9 1.9 copy-start.4
  241.8 3.1 %copy-start.5 = (f32[1,1536]{1,0:T(1,128)S(1)}, f32[1,1536]{1,0:T(1,128)}, u32[]{:S(2)}) copy-start(f32[1,1536]{1,0:T(1,128)} %get-tuple-element.8) | copy-start | bytes 18436
  241.8 3.7 %copy-start = (bf16[256,2048]{1,0:T(8,128)(2,1)S(1)}, bf16[256,2048]{1,0:T(8,128)(2,1)}, u32[]{:S(2)}) copy-start(bf16[256,2048]{1,0:T(8,128)(2,1)} %get-tuple-element.21) | copy-start | bytes 3145732

commit v4 on v3

--- a/solution.py
+++ b/solution.py
@@ -11,7 +11,7 @@
 f32, bf16 = jnp.float32, jnp.bfloat16
 
 
-def kernel(sizes, tok, mid, cot, w1, v1, w2, v2, out, grad, norms, full1, downs1, full2, downs2, toks, mids, cots, mgs, xb, hidden, d_gate, d_up, mgt, gates, uppers, part, got1, snd2, got2, dn, rs_out, rs_in, gb, nb, w_send, w_recv, own_sem, x_send, x_recv, s1_send, s1_recv, s2_send, s2_recv, s3_send, s3_recv, r_send, r_recv, g_send, g_recv, n_send, n_recv):
+def kernel(sizes, tok, mid, cot, g1, u1, v1, g2, u2, v2, out, grad, norms, full1, downs1, full2, downs2, toks, mids, cots, mgs, xb, hidden, d_gate, d_up, mgt, gates, uppers, part, got1, snd2, got2, dn, rs_out, rs_in, gb, nb, w_send, w_recv, own_sem, x_send, x_recv, s1_send, s1_recv, s2_send, s2_recv, s3_send, s3_recv, r_send, r_recv, g_send, g_recv, n_send, n_recv):
     R, F, T, n, D, H, pieces = sizes
     S, half, C, width = D // F, D // F // 2, D // T, H // pieces
     both = 2 if pieces > 1 else 1
@@ -78,7 +78,17 @@
     mine = pl.ds(pl.multiple_of(r * n, n), n)
     pairs = (mids, cots, toks, mgs)
     held = pl.ds(pl.multiple_of(f * S, S), S)
-    loads = [pltpu.make_async_copy(src, dst, own_sem.at[i]) for i, (src, dst) in enumerate(((w2, full2.at[held]), (mid, mids.at[mine]), (cot, cots.at[mine]), (tok, toks.at[mine]), (v2, downs2.at[held]), (w1, full1.at[held]), (v1, downs1.at[held])))]
+    def pair_loads(g, u, full):
+        if H % 128 > 0:
+            return [(g, full.at[held])]
+        taken = pl.ds(pl.multiple_of(r * H, 128), H)
+        return [(g.at[:, taken], full.at[held, pl.ds(0, H)]), (u.at[:, taken], full.at[held, pl.ds(H, H)])]
+
+    wanted = pair_loads(g2, u2, full2)
+    ahead = len(wanted)
+    wanted += [(mid, mids.at[mine]), (cot, cots.at[mine]), (tok, toks.at[mine]), (v2, downs2.at[held]), (v1, downs1.at[held])]
+    wanted += pair_loads(g1, u1, full1)
+    loads = [pltpu.make_async_copy(src, dst, own_sem.at[i]) for i, (src, dst) in enumerate(wanted)]
     for c in loads:
         c.start()
 
@@ -90,13 +100,14 @@
             rows = pl.ds(pl.multiple_of(lax.rem(r + R - k, R) * n, n), n)
             remote(pairs[i].at[rows], pairs[i].at[rows], x_send.at[i, k - 1], x_recv.at[i, k - 1], rep=lax.rem(r + k, R)).wait_recv()
 
-    loads[0].wait()
+    for c in loads[:ahead]:
+        c.wait()
     start_ring(second_gu)
     for i in range(3):
-        loads[i + 1].wait()
+        loads[ahead + i].wait()
         for c in swap(i):
             c.start()
-    for c in loads[4:]:
+    for c in loads[ahead + 3 :]:
         c.wait()
 
     def normalise(pair):
@@ -340,8 +351,11 @@
     start = lax.axis_index("rep") * H
 
     def own(gate_w, up_w, down_w):
+        down = lax.dynamic_slice_in_dim(down_w, start, H, 0).T
+        if H % 128 == 0:
+            return gate_w, up_w, down
         pair = [lax.dynamic_slice_in_dim(w, start, H, 1) for w in (gate_w, up_w)]
-        return jnp.concatenate(pair, axis=1), lax.dynamic_slice_in_dim(down_w, start, H, 0).T
+        return jnp.concatenate(pair, axis=1), up_w, down
 
     dma = pltpu.SemaphoreType.DMA
     m = R * n
@@ -354,7 +368,7 @@
             jax.ShapeDtypeStruct((S, R * H), f32),
             jax.ShapeDtypeStruct((1, R * H), f32),
         ),
-        in_specs=[any_space] * 7,
+        in_specs=[any_space] * 9,
         out_specs=(vmem, vmem, vmem),
         scratch_shapes=[
             pltpu.VMEM((D, 2 * H), bf16),
@@ -383,7 +397,7 @@
             pltpu.VMEM((F, 1, R * H), f32),
             dma((2, 2, 2)),
             dma((2, 2, F - 1, pieces + (2 if pieces > 1 else 1))),
-            dma((7,)),
+            dma((9,)),
             dma((4, R - 1)),
             dma((4, R - 1)),
             dma((2, T - 1)),

time: 247 us -> 244 us (0.988)
    unnamed x16 -> x8, local copies, waits for them, and re-layouts: 5.95 us -> 5.93 us
where the time goes in v4:
time: 244 us
  Pallas kernels  236 us (97%)
  local copies, waits for them, and re-layouts  7.1 us (3%)
    pallas_call x1, Pallas kernels, on_device(): pl.pallas_call(functools.partial(kernel, sizes), out_shape=(jax.ShapeDtyp...  236 us
    unnamed x8, local copies, waits for them, and re-layouts  5.93 us

profile of v4, /device:TPU:0, one launch (start us, length us, event | category | flops | bytes accessed | tf_op | source)
XLA Modules:
  0.0 244.3 jit_solution(9462708712932138181)
XLA Ops:
  0.6 1.2 constant_dynamic-slice_fusion
  1.8 0.9 copy.16
  2.7 0.9 copy.15
  3.6 235.9 %shard_map.112 = (bf16[256,2048]{1,0:T(8,128)(2,1)}, f32[256,1536]{1,0:T(8,128)}, f32[1,1536]{1,0:T(1,128)}) custom-call(bf16[256,2048]{1,0:T(8,128)(2,1)} %tok.1, bf16[256,2048]{1,0:T(8,128)(2,1)} %mid.1, bf16[256,2048]{1,0:T(8,128)(2,1)} %cot.1, bf16[256,1536]{1,0:T(8,128)(2,1)} %g1.1, bf16[256,1536]{1,0:T(8,128)(2,1)} %u1_.1, bf16[256,768]{1,0:T(8,128)(2,1)} %bitcast.5, ...), custom_call_target="tpu_custom_call" | custom-call | tf_op jit(solution)/shard_map/pallas_call | solution.py:364
  239.6 0.0 copy-start.1
  239.6 0.0 copy-start
  239.6 3.1 %copy.14 = f32[1536,256]{1,0:T(8,128)} copy(f32[1536,256]{0,1:T(8,128)} %bitcast.3) | data formatting | bytes 3145728
  242.7 0.0 copy-done.1
  242.7 0.6 reduce
  243.4 0.0 copy-done
  243.4 1.0 copy.18
Async XLA Ops:
  239.6 3.1 %copy-start.1 = (f32[1,1536]{1,0:T(1,128)S(1)}, f32[1,1536]{1,0:T(1,128)}, u32[]{:S(2)}) copy-start(f32[1,1536]{1,0:T(1,128)} %get-tuple-element.8) | copy-start | bytes 18436
  239.6 3.7 %copy-start = (bf16[256,2048]{1,0:T(8,128)(2,1)S(1)}, bf16[256,2048]{1,0:T(8,128)(2,1)}, u32[]{:S(2)}) copy-start(bf16[256,2048]{1,0:T(8,128)(2,1)} %get-tuple-element.17) | copy-start | bytes 3145732
